TPU v7x, 32 devices: a whole 2x2x4 slice. The times are simulated.
32 devices in a mesh: fs: 16 (over z, y, x), tp: 2 (over core).
Axes of the slice: x: 2, y: 2, z: 4, core: 2. Of those that a mesh axis runs over, the one named last changes fastest.
Arguments:
- normed_input: bfloat16 [8192, 2048], P('fs', 'tp'), may hold values from -6 to 6
- cotangent: bfloat16 [8192, 2048], P('fs', 'tp'), may hold values from -6 to 6
- up_weight: bfloat16 [2048, 8192], P('fs', 'tp'), may hold values from -0.125 to 0.125
- down_weight: bfloat16 [8192, 2048], P('tp', 'fs'), may hold values from -0.0625 to 0.0625
Outputs:
- input_grad: bfloat16 [8192, 2048], P('fs', 'tp')
- up_grad: float32 [2048, 8192], P('fs', 'tp')
- down_grad: float32 [8192, 2048], P('tp', 'fs')
All inputs are finite; a program needn't handle non-finite values.
Results may differ from a plain program's by a relative error of at most 0.018.
Values may be sent and summed in bfloat16 or wider, within the bound.
A program may use at most 192 MiB of HBM per device.

v0:
```python
import jax
import jax.numpy as jnp
from jax import lax
from jax.sharding import PartitionSpec as P


def right_product(left, right):
    return lax.dot_general(
        left, right, (((1,), (1,)), ((), ())), preferred_element_type=jnp.float32
    )


def left_product(left, right):
    return lax.dot_general(
        left, right, (((0,), (0,)), ((), ())), preferred_element_type=jnp.float32
    )


def per_device(normed_input, cotangent, up_weight, down_weight):
    whole_input, whole_cot = (
        lax.all_gather(normed_input, "tp", axis=1, tiled=True),
        lax.all_gather(cotangent, "tp", axis=1, tiled=True),
    )
    rows = whole_input.shape[0]
    tokens = rows * lax.axis_size("fs")
    scale = lax.rsqrt(jnp.asarray(tokens, jnp.float32))
    block = whole_cot
    act_grad = right_product(block, lax.all_gather(down_weight, "fs", axis=1, tiled=True))
    whole_up = lax.all_gather(up_weight, "fs", axis=0, tiled=True)
    pre = jnp.dot(whole_input, whole_up, preferred_element_type=jnp.float32)
    rectified = jax.nn.relu(pre)
    act = (rectified * rectified).astype(jnp.bfloat16)
    pre_grad = (2.0 * rectified * act_grad).astype(jnp.bfloat16)
    partial_value = right_product(pre_grad, whole_up)
    input_grad = lax.psum_scatter(
        partial_value.astype(jnp.bfloat16), "tp", scatter_dimension=1, tiled=True
    )
    block = whole_input
    up_grad = lax.psum_scatter(
        (left_product(block, pre_grad) * scale).astype(jnp.bfloat16),
        "fs",
        scatter_dimension=0,
        tiled=True,
    ).astype(jnp.float32)
    down_term = left_product(act, whole_cot) * scale
    down_grad = lax.psum_scatter(
        down_term.astype(jnp.bfloat16), "fs", scatter_dimension=1, tiled=True
    ).astype(jnp.float32)
    return (input_grad, up_grad, down_grad)


def solution(mesh):
    in_specs = (P("fs", "tp"), P("fs", "tp"), P("fs", "tp"), P("tp", "fs"))
    out_specs = (P("fs", "tp"), P("fs", "tp"), P("tp", "fs"))
    return jax.shard_map(
        per_device, mesh=mesh, in_specs=in_specs, out_specs=out_specs, check_vma=False
    )
```

profile of v0, /device:TPU:0, one launch (start us, length us, event | category | flops | bytes accessed | tf_op | source)
XLA Modules:
  0.0 1207.0 jit_solution(5225547359864163482)
XLA Ops:
  7.2 0.0 all-gather.5.cloned.1.call-start
  7.2 0.7 all-gather.5.cloned.1.call-update
  7.9 0.0 all-gather.7.cloned.1.call-start
  7.9 0.7 all-gather.7.cloned.1.call-update
  8.6 0.0 all-gather.9.cloned.1.call-start
  8.7 0.7 all-gather.9.cloned.1.call-update
  9.4 0.0 all-gather.11.cloned.1.call-start
  9.4 0.5 all-gather.11.cloned.1.call-update
  10.0 0.0 reduce-scatter.12.cloned.1.call-start
  10.0 12.8 %all-gather.5.cloned.1.call-done = bf16[512,2048]{1,0:T(8,128)(2,1)} async-done(((bf16[512,1024]{1,0:T(8,128)(2,1)}), bf16[512,2048]{1,0:T(8,128)(2,1)}) %all-gather.5.cloned.1.call-update) | async-done | bytes 2097168 | tf_op jit(solution)/shard_map/all_gather | solution.py:21
  22.8 195.0 %all-gather.7.cloned.1.call-done = bf16[2048,4096]{1,0:T(8,128)(2,1)} async-done(((bf16[128,4096]{1,0:T(8,128)(2,1)}), bf16[2048,4096]{1,0:T(8,128)(2,1)}) %all-gather.7.cloned.1.call-update) | async-done | bytes 16777232 | tf_op jit(solution)/shard_map/all_gather | solution.py:29
  217.8 14.9 %fusion.3 = f32[512,4096]{1,0:T(8,128)} fusion(bf16[512,2048]{1,0:T(8,128)(2,1)} %all-gather.5.cloned.1.call-done, bf16[2048,4096]{1,0:T(8,128)(2,1)} %all-gather.7.cloned.1.call-done), kind=kOutput, calls=%fused_computation.8 | convolution fusion | flops 8589934592 | bytes 27262976 | tf_op jit(solution)/shard_map/dot_general | solution.py:30
  232.7 0.0 all-gather.9.cloned.1.call-done
  232.7 16.2 %multiply_convert_fusion = bf16[4096,2048]{1,0:T(8,128)(2,1)} fusion(bf16[512,2048]{1,0:T(8,128)(2,1)} %all-gather.9.cloned.1.call-done, f32[512,4096]{1,0:T(8,128)} %fusion.3), kind=kOutput, calls=%fused_computation | convolution fusion | flops 8613003264 | bytes 27262976 | tf_op jit(solution)/shard_map/dot_general | solution.py:14
  248.9 21.5 %copy.11 = bf16[4096,2048]{0,1:T(8,128)(2,1)} copy(bf16[4096,2048]{1,0:T(8,128)(2,1)} %multiply_convert_fusion) | data formatting | bytes 33554432
  270.4 0.0 reduce-scatter.12.cloned.1.call-update
  270.5 0.0 copy-start
  270.5 0.2 reduce-scatter.10.cloned.1.call-start
  270.7 210.3 %all-gather.11.cloned.1.call-done = bf16[4096,2048]{1,0:T(8,128)(2,1)} async-done(((bf16[4096,128]{1,0:T(8,128)(2,1)}), bf16[4096,2048]{1,0:T(8,128)(2,1)}) %all-gather.11.cloned.1.call-update) | async-done | bytes 16777232 | tf_op jit(solution)/shard_map/all_gather | solution.py:28
  481.0 15.6 %multiply_convert_fusion.3 = bf16[512,4096]{1,0:T(8,128)(2,1)} fusion(f32[512,4096]{1,0:T(8,128)} %fusion.3, bf16[512,2048]{1,0:T(8,128)(2,1)} %all-gather.9.cloned.1.call-done, bf16[4096,2048]{1,0:T(8,128)(2,1)} %all-gather.11.cloned.1.call-done), kind=kOutput, calls=%fused_computation.4 | convolution fusion | flops 8598323200 | bytes 31457280 | tf_op jit(solution)/shard_map/dot_general | solution.py:8
  496.6 0.0 copy-done
  496.6 14.8 %fusion = bf16[2048,4096]{0,1:T(8,128)(2,1)} fusion(bf16[512,4096]{1,0:T(8,128)(2,1)} %multiply_convert_fusion.3, bf16[512,2048]{1,0:T(8,128)(2,1)S(1)} %copy-done), kind=kOutput, calls=%fused_computation.2 | convolution fusion | flops 8606711808 | bytes 23068672 | tf_op jit(solution)/shard_map/dot_general | solution.py:14
  511.4 21.4 %copy.9 = bf16[2048,4096]{1,0:T(8,128)(2,1)} copy(bf16[2048,4096]{0,1:T(8,128)(2,1)} %fusion) | data formatting | bytes 33554432
  532.8 0.0 reduce-scatter.10.cloned.1.call-update
  532.8 0.3 reduce-scatter.8.cloned.1.call-start
  533.1 14.8 %convolution_convert_fusion = bf16[512,2048]{1,0:T(8,128)(2,1)} fusion(bf16[512,4096]{1,0:T(8,128)(2,1)} %multiply_convert_fusion.3, bf16[2048,4096]{1,0:T(8,128)(2,1)} %all-gather.7.cloned.1.call-done), kind=kOutput, calls=%fused_computation.6 | convolution fusion | flops 8590983168 | bytes 23068672 | tf_op jit(solution)/shard_map/dot_general | solution.py:8
  547.9 0.0 reduce-scatter.8.cloned.1.call-update
  547.9 279.9 %reduce-scatter.12.cloned.1.call-done = bf16[128,4096]{1,0:T(8,128)(2,1)} async-done(((bf16[2048,4096]{1,0:T(8,128)(2,1)}), bf16[128,4096]{1,0:T(8,128)(2,1)}) %reduce-scatter.12.cloned.1.call-update) | async-done | bytes 1048592
  827.8 1.6 copy.12
  829.4 1.5 convert_element_type.31
  830.9 351.1 %reduce-scatter.10.cloned.1.call-done = bf16[128,4096]{1,0:T(8,128)(2,1)} async-done(((bf16[2048,4096]{1,0:T(8,128)(2,1)}), bf16[128,4096]{1,0:T(8,128)(2,1)}) %reduce-scatter.10.cloned.1.call-update) | async-done | bytes 1048592
  1182.0 1.6 copy.10
  1183.6 1.6 copy.8
  1185.3 14.9 %reduce-scatter.8.cloned.1.call-done = bf16[512,1024]{1,0:T(8,128)(2,1)} async-done(((bf16[512,2048]{1,0:T(8,128)(2,1)}), bf16[512,1024]{1,0:T(8,128)(2,1)}) %reduce-scatter.8.cloned.1.call-update) | async-done | bytes 1048592 | tf_op jit(solution)/shard_map/reduce_scatter | solution.py:35
Async XLA Ops:
  7.2 15.7 %all-gather.5.cloned.1.call-start = ((), (), s32[]{:S(2)}) async-start(), calls=%async_computation.3 | async-start | bytes 3145728 | tf_op jit(solution)/shard_map/all_gather | solution.py:21
  7.9 209.9 %all-gather.7.cloned.1.call-start = ((), (), s32[]{:S(2)}) async-start(), calls=%async_computation.4 | async-start | bytes 17825792 | tf_op jit(solution)/shard_map/all_gather | solution.py:29
  8.6 224.1 %all-gather.9.cloned.1.call-start = ((), (), s32[]{:S(2)}) async-start(), calls=%async_computation.5 | async-start | bytes 3145728 | tf_op jit(solution)/shard_map/all_gather | solution.py:22
  9.4 471.7 %all-gather.11.cloned.1.call-start = ((), (), s32[]{:S(2)}) async-start(), calls=%async_computation.6 | async-start | bytes 17825792 | tf_op jit(solution)/shard_map/all_gather | solution.py:28
  10.0 817.9 %reduce-scatter.12.cloned.1.call-start = ((), (), s32[]{:S(2)}) async-start(), calls=%async_computation.9 | async-start | bytes 17825792
  270.5 226.2 %copy-start = (bf16[512,2048]{1,0:T(8,128)(2,1)S(1)}, bf16[512,2048]{1,0:T(8,128)(2,1)}, u32[]{:S(2)}) copy-start(bf16[512,2048]{1,0:T(8,128)(2,1)} %all-gather.5.cloned.1.call-done) | copy-start | bytes 6291460
  270.5 911.5 %reduce-scatter.10.cloned.1.call-start = ((), (), s32[]{:S(2)}) async-start(), calls=%async_computation.8 | async-start | bytes 17825792
  532.8 667.3 %reduce-scatter.8.cloned.1.call-start = ((), (), s32[]{:S(2)}) async-start(), calls=%async_computation.7 | async-start | bytes 3145728 | tf_op jit(solution)/shard_map/reduce_scatter | solution.py:35
Sparse Core Ops, SparseCore 0:
  9.5 13.2 all-gather.4
  25.6 192.1 all-gather.6
  219.4 8.7 all-gather.8
  230.7 250.2 all-gather.10
  483.2 344.5 reduce-scatter.11
  830.0 352.0 reduce-scatter.9
  1184.8 15.2 reduce-scatter.7
where the time goes:
time: 1210 us
  waiting for transfers between devices  1070 us (88%)
  matrix products  76.2 us (6%)
  local copies, waits for them, and re-layouts  47.8 us (4%)
  between operations  14.2 us (1%)
    unnamed x9, waiting for transfers between devices  634 us
    all_gather x1, waiting for transfers between devices, per_device(): lax.all_gather(down_weight, 'fs', axis=1, tiled=True)  210 us
    all_gather x1, waiting for transfers between devices, per_device(): whole_up = lax.all_gather(up_weight, 'fs', axis=0, tiled=True)  195 us
    unnamed x7, local copies, waits for them, and re-layouts  47.8 us
    dot_general x2, matrix products, left_product(): lax.dot_general(left, right, (((0,), (0,)), ((), ())), preferred_element_...  30.9 us
    dot_general x2, matrix products, right_product(): lax.dot_general(left, right, (((1,), (1,)), ((), ())), preferred_element_...  30.4 us
  transfers between devices with their start and end apart: 7, of which 6 were waited for; matrix products, arithmetic and copies ran while one was open for 10% of the time, Pallas kernels for 0%

commit v1 on v0

--- a/solution.py
+++ b/solution.py
@@ -25,7 +25,7 @@
     tokens = rows * lax.axis_size("fs")
     scale = lax.rsqrt(jnp.asarray(tokens, jnp.float32))
     block = whole_cot
-    act_grad = right_product(block, lax.all_gather(down_weight, "fs", axis=1, tiled=True))
+    act_grad = right_product(block, jnp.concatenate(lax.all_gather(down_weight, "fs"), axis=1))
     whole_up = lax.all_gather(up_weight, "fs", axis=0, tiled=True)
     pre = jnp.dot(whole_input, whole_up, preferred_element_type=jnp.float32)
     rectified = jax.nn.relu(pre)

time: 1210 us -> 1150 us (0.950)
  waiting for transfers between devices: 1070 us -> 991 us
  local copies, waits for them, and re-layouts: 47.8 us -> 69.5 us
    all_gather x1, waiting for transfers between devices: 210 us -> 153 us  [per_device(): lax.all_gather(down_weight, 'fs')]
    reshape x0 -> x1, local copies, waits for them, and re-layouts: none -> 21.3 us  [per_device(): jnp.concatenate(lax.all_gather(down_weight, 'fs'), axis=1)]
    unnamed x9, waiting for transfers between devices: 634 us -> 615 us
    unnamed x7 -> x11, local copies, waits for them, and re-layouts: 47.8 us -> 48.3 us
  transfers between devices with their start and end apart: 7 -> 7, of which waited for: 6 -> 6; matrix products, arithmetic and copies ran while one was open for 10% -> 12% of each run, Pallas kernels for 0% -> 0%
where the time goes in v1:
time: 1150 us
  waiting for transfers between devices  991 us (86%)
  matrix products  72.2 us (6%)
  local copies, waits for them, and re-layouts  69.5 us (6%)
  between operations  14.2 us (1%)
    unnamed x9, waiting for transfers between devices  615 us
    all_gather x1, waiting for transfers between devices, per_device(): whole_up = lax.all_gather(up_weight, 'fs', axis=0, tiled=True)  195 us
    all_gather x1, waiting for transfers between devices, per_device(): lax.all_gather(down_weight, 'fs')  153 us
    unnamed x11, local copies, waits for them, and re-layouts  48.3 us
    dot_general x2, matrix products, left_product(): lax.dot_general(left, right, (((0,), (0,)), ((), ())), preferred_element_...  28.6 us
    dot_general x2, matrix products, right_product(): lax.dot_general(left, right, (((1,), (1,)), ((), ())), preferred_element_...  28.5 us
  transfers between devices with their start and end apart: 7, of which 6 were waited for; matrix products, arithmetic and copies ran while one was open for 12% of the time, Pallas kernels for 0%

profile of v1, /device:TPU:0, one launch (start us, length us, event | category | flops | bytes accessed | tf_op | source)
XLA Modules:
  0.0 1148.9 jit_solution(9772851425815069178)
XLA Ops:
  7.2 0.0 all-gather.6.cloned.1.call-start
  7.2 0.7 all-gather.6.cloned.1.call-update
  7.9 0.0 all-gather.8.cloned.1.call-start
  7.9 0.7 all-gather.8.cloned.1.call-update
  8.6 0.0 all-gather.10.cloned.1.call-start
  8.7 0.7 all-gather.10.cloned.1.call-update
  9.4 0.0 all-gather.12.cloned.1.call-start
  9.4 0.5 all-gather.12.cloned.1.call-update
  10.0 0.0 reduce-scatter.12.cloned.1.call-start
  10.0 12.8 %all-gather.6.cloned.1.call-done = bf16[512,2048]{1,0:T(8,128)(2,1)} async-done(((bf16[512,1024]{1,0:T(8,128)(2,1)}), bf16[512,2048]{1,0:T(8,128)(2,1)}) %all-gather.6.cloned.1.call-update) | async-done | bytes 2097168 | tf_op jit(solution)/shard_map/all_gather | solution.py:21
  22.8 195.0 %all-gather.8.cloned.1.call-done = bf16[2048,4096]{1,0:T(8,128)(2,1)} async-done(((bf16[128,4096]{1,0:T(8,128)(2,1)}), bf16[2048,4096]{1,0:T(8,128)(2,1)}) %all-gather.8.cloned.1.call-update) | async-done | bytes 16777232 | tf_op jit(solution)/shard_map/all_gather | solution.py:29
  217.8 15.0 %fusion.3 = f32[512,4096]{1,0:T(8,128)} fusion(bf16[512,2048]{1,0:T(8,128)(2,1)} %all-gather.6.cloned.1.call-done, bf16[2048,4096]{1,0:T(8,128)(2,1)} %all-gather.8.cloned.1.call-done), kind=kOutput, calls=%fused_computation.8 | convolution fusion | flops 8589934592 | bytes 27262976 | tf_op jit(solution)/shard_map/dot_general | solution.py:30
  232.8 0.0 all-gather.10.cloned.1.call-done
  232.8 16.2 %multiply_convert_fusion = bf16[4096,2048]{1,0:T(8,128)(2,1)} fusion(bf16[512,2048]{1,0:T(8,128)(2,1)} %all-gather.10.cloned.1.call-done, f32[512,4096]{1,0:T(8,128)} %fusion.3), kind=kOutput, calls=%fused_computation | convolution fusion | flops 8613003264 | bytes 27262976 | tf_op jit(solution)/shard_map/dot_general | solution.py:14
  249.0 20.7 %copy.15 = bf16[4096,2048]{0,1:T(8,128)(2,1)} copy(bf16[4096,2048]{1,0:T(8,128)(2,1)} %multiply_convert_fusion) | data formatting | bytes 33554432
  269.7 0.0 reduce-scatter.12.cloned.1.call-update
  269.7 0.2 reduce-scatter.10.cloned.1.call-start
  269.9 153.1 %all-gather.12.cloned.1.call-done = bf16[65536,128]{1,0:T(8,128)(2,1)} async-done(((bf16[4096,128]{1,0:T(8,128)(2,1)}), bf16[65536,128]{1,0:T(8,128)(2,1)}) %all-gather.12.cloned.1.call-update) | async-done | bytes 16777232 | tf_op jit(solution)/shard_map/all_gather | solution.py:28
  423.0 0.0 copy-start.1
  423.0 21.3 %copy.11 = bf16[4096,16,128]{0,2,1:T(8,128)(2,1)} copy(bf16[4096,16,128]{2,0,1:T(8,128)(2,1)} %bitcast.19) | data formatting | bytes 33554432 | tf_op jit(solution)/shard_map/reshape | solution.py:28
  444.3 0.0 copy-done.1
  444.3 0.0 copy-start
  444.3 13.8 %multiply_convert_fusion.3 = bf16[512,4096]{1,0:T(8,128)(2,1)S(1)} fusion(f32[512,4096]{1,0:T(8,128)} %fusion.3, bf16[512,2048]{1,0:T(8,128)(2,1)S(1)} %copy-done.1, bf16[4096,2048]{0,1:T(8,128)(2,1)} %bitcast.20), kind=kOutput, calls=%fused_computation.4 | convolution fusion | flops 8598323200 | bytes 31457280 | tf_op jit(solution)/shard_map/dot_general | solution.py:8
  458.0 0.0 copy-start.2
  458.1 2.0 copy-done.2
  460.0 0.0 copy-done
  460.1 12.4 %fusion = bf16[2048,4096]{0,1:T(8,128)(2,1)} fusion(bf16[512,4096]{1,0:T(8,128)(2,1)S(1)} %multiply_convert_fusion.3, bf16[512,2048]{1,0:T(8,128)(2,1)S(1)} %copy-done), kind=kOutput, calls=%fused_computation.2 | convolution fusion | flops 8606711808 | bytes 23068672 | tf_op jit(solution)/shard_map/dot_general | solution.py:14
  472.5 20.8 %copy.13 = bf16[2048,4096]{1,0:T(8,128)(2,1)} copy(bf16[2048,4096]{0,1:T(8,128)(2,1)} %fusion) | data formatting | bytes 33554432
  493.3 0.0 reduce-scatter.10.cloned.1.call-update
  493.3 0.3 reduce-scatter.8.cloned.1.call-start
  493.6 14.8 %convolution_convert_fusion = bf16[512,2048]{1,0:T(8,128)(2,1)} fusion(bf16[512,4096]{1,0:T(8,128)(2,1)} %copy-done.2, bf16[2048,4096]{1,0:T(8,128)(2,1)} %all-gather.8.cloned.1.call-done), kind=kOutput, calls=%fused_computation.6 | convolution fusion | flops 8590983168 | bytes 23068672 | tf_op jit(solution)/shard_map/dot_general | solution.py:8
  508.3 0.0 reduce-scatter.8.cloned.1.call-update
  508.4 261.4 %reduce-scatter.12.cloned.1.call-done = bf16[128,4096]{1,0:T(8,128)(2,1)} async-done(((bf16[2048,4096]{1,0:T(8,128)(2,1)}), bf16[128,4096]{1,0:T(8,128)(2,1)}) %reduce-scatter.12.cloned.1.call-update) | async-done | bytes 1048592
  769.8 1.6 copy.16
  771.4 1.5 convert_element_type.31
  772.8 351.2 %reduce-scatter.10.cloned.1.call-done = bf16[128,4096]{1,0:T(8,128)(2,1)} async-done(((bf16[2048,4096]{1,0:T(8,128)(2,1)}), bf16[128,4096]{1,0:T(8,128)(2,1)}) %reduce-scatter.10.cloned.1.call-update) | async-done | bytes 1048592
  1124.0 1.6 copy.14
  1125.6 1.6 copy.12
  1127.2 14.9 %reduce-scatter.8.cloned.1.call-done = bf16[512,1024]{1,0:T(8,128)(2,1)} async-done(((bf16[512,2048]{1,0:T(8,128)(2,1)}), bf16[512,1024]{1,0:T(8,128)(2,1)}) %reduce-scatter.8.cloned.1.call-update) | async-done | bytes 1048592 | tf_op jit(solution)/shard_map/reduce_scatter | solution.py:35
Async XLA Ops:
  7.2 15.7 %all-gather.6.cloned.1.call-start = ((), (), s32[]{:S(2)}) async-start(), calls=%async_computation.3 | async-start | bytes 3145728 | tf_op jit(solution)/shard_map/all_gather | solution.py:21
  7.9 209.9 %all-gather.8.cloned.1.call-start = ((), (), s32[]{:S(2)}) async-start(), calls=%async_computation.4 | async-start | bytes 17825792 | tf_op jit(solution)/shard_map/all_gather | solution.py:29
  8.6 224.1 %all-gather.10.cloned.1.call-start = ((), (), s32[]{:S(2)}) async-start(), calls=%async_computation.5 | async-start | bytes 3145728 | tf_op jit(solution)/shard_map/all_gather | solution.py:22
  9.4 413.6 %all-gather.12.cloned.1.call-start = ((), (), s32[]{:S(2)}) async-start(), calls=%async_computation.7 | async-start | bytes 17825792 | tf_op jit(solution)/shard_map/all_gather | solution.py:28
  10.0 759.8 %reduce-scatter.12.cloned.1.call-start = ((), (), s32[]{:S(2)}) async-start(), calls=%async_computation.9 | async-start | bytes 17825792
  269.7 854.3 %reduce-scatter.10.cloned.1.call-start = ((), (), s32[]{:S(2)}) async-start(), calls=%async_computation.8 | async-start | bytes 17825792
  423.0 21.3 %copy-start.1 = (bf16[512,2048]{1,0:T(8,128)(2,1)S(1)}, bf16[512,2048]{1,0:T(8,128)(2,1)}, u32[]{:S(2)}) copy-start(bf16[512,2048]{1,0:T(8,128)(2,1)} %all-gather.10.cloned.1.call-done) | copy-start | bytes 6291460
  444.3 15.8 %copy-start = (bf16[512,2048]{1,0:T(8,128)(2,1)S(1)}, bf16[512,2048]{1,0:T(8,128)(2,1)}, u32[]{:S(2)}) copy-start(bf16[512,2048]{1,0:T(8,128)(2,1)} %all-gather.6.cloned.1.call-done) | copy-start | bytes 6291460
  458.0 2.0 copy-start.2
  493.3 648.8 %reduce-scatter.8.cloned.1.call-start = ((), (), s32[]{:S(2)}) async-start(), calls=%async_computation.6 | async-start | bytes 3145728 | tf_op jit(solution)/shard_map/reduce_scatter | solution.py:35
Sparse Core Ops, SparseCore 0:
  9.5 13.2 all-gather.5
  25.6 192.1 all-gather.7
  219.4 8.7 all-gather.9
  230.8 192.1 all-gather.11
  425.1 344.5 reduce-scatter.11
  771.9 352.0 reduce-scatter.9
  1126.8 15.2 reduce-scatter.7
